TPU v7x, 32 devices: a whole 2x2x4 slice. The times are simulated.
32 devices in a mesh: grp: 2 (over y), fs: 4 (over z), tp: 4 (over x, core).
Axes of the slice: x: 2, y: 2, z: 4, core: 2. Of those that a mesh axis runs over, the one named last changes fastest.
Arguments:
- tokens: bfloat16 [1792, 2048], P(('grp', 'fs'), 'tp'), parts along dimension 0, may hold values from -6 to 6
- route_ids: int32 [1792, 2], P(('grp', 'fs')), parts along dimension 0, may hold values from 0 to 3, all different within a row; in each aligned block of 224 rows (0 to 223, 224 to 447, ...) at most 168 rows name the same one
- route_weights: float32 [1792, 2], P(('grp', 'fs')), parts along dimension 0, may hold values from 0.25 to 1
- norm_gain: float32 [2048], P('fs'), may hold values from 0.1 to 1.9
- gate_master: float32 [4, 2048, 512], P(None, 'fs', 'tp'), may hold values from -0.125 to 0.125
- up_master: float32 [4, 2048, 512], P(None, 'fs', 'tp'), may hold values from -0.125 to 0.125
- down_master: float32 [4, 2048, 512], P(None, 'fs', 'tp'), may hold values from -0.25 to 0.25
Outputs:
- gate_serve: bfloat16 [8, 2048, 512], P(('grp', 'fs'), None, 'tp'), parts along dimension 0
- up_serve: bfloat16 [8, 2048, 512], P(('grp', 'fs'), None, 'tp'), parts along dimension 0
- down_serve: bfloat16 [8, 2048, 512], P(('grp', 'fs'), None, 'tp'), parts along dimension 0
- moe_output: bfloat16 [1792, 2048], P(('grp', 'fs'), 'tp'), parts along dimension 0
There are 2 independent parts, one for each index of `grp`. A program takes and returns all parts, laid end to end along the dimension named above; an argument that names none is the same for every part. Nothing has to cross between parts.
Inputs may be any that keep to these rules, and one draw needn't show every extreme that they name: `route_ids`: the 2 experts of a row differ; within the rows of one index of fs (aligned blocks of 224 rows) no expert is named more than 168 times.
All inputs are finite; a program needn't handle non-finite values.
Results may differ from a plain program's by a relative error of at most 0.012.
Values may be sent and summed in bfloat16 or wider, within the bound.
A program may use at most 64 MiB of HBM per device.

v0:
```python
import functools
import jax
import jax.numpy as jnp
from jax import lax
from jax.experimental import pallas as pl
from jax.experimental.pallas import tpu as pltpu
from jax.sharding import PartitionSpec as P

norm_epsilon = 1e-06


def slot_numbers(route_ids, experts, capacity):
    flat_ids = route_ids.reshape(-1)
    onehot = (flat_ids[:, None] == jnp.arange(experts, dtype=jnp.int32)[None, :]).astype(jnp.int32)
    before = jnp.cumsum(onehot, axis=0) - onehot
    position = jnp.sum(before * onehot, axis=1)
    return (flat_ids * capacity + position).reshape(route_ids.shape)


def local(tokens, route_ids, route_weights, norm_gain, gate_master, up_master, down_master):
    experts = gate_master.shape[0]
    shards = lax.axis_size("fs")
    columns = lax.axis_size("tp")
    per_device = experts // shards
    tok_rows = route_ids.shape[0]
    top_count = route_ids.shape[1]
    local_width = tokens.shape[1]
    model_width = local_width * columns
    capacity = max(2, 3 * tok_rows * top_count // (2 * experts))
    row_gain = norm_gain[None, :, None]
    gate_half = (gate_master * row_gain).astype(jnp.bfloat16)
    up_half = (up_master * row_gain).astype(jnp.bfloat16)
    down_half = down_master.astype(jnp.bfloat16)
    gate_serve, up_serve, down_serve = (
        lax.all_to_all(gate_half, "fs", split_axis=0, concat_axis=1, tiled=True),
        lax.all_to_all(up_half, "fs", split_axis=0, concat_axis=1, tiled=True),
        lax.all_to_all(down_half, "fs", split_axis=0, concat_axis=1, tiled=True),
    )
    slot_ids = slot_numbers(route_ids, experts, capacity)
    slot_range = jnp.arange(experts * capacity, dtype=jnp.int32)
    selects = [
        (slot_ids[:, rank_slot, None] == slot_range[None, :]).astype(jnp.bfloat16)
        for rank_slot in range(top_count)
    ]
    placing = selects[0]
    for extra in selects[1:]:
        placing = placing + extra
    local_values = tokens.astype(jnp.float32)
    squares = lax.psum(jnp.sum(local_values * local_values, axis=1), "tp")
    inverse = lax.rsqrt(squares / model_width + norm_epsilon)[:, None]
    normed = (local_values * inverse).astype(jnp.bfloat16)
    buffer = jnp.einsum("ts,td->sd", placing, normed, preferred_element_type=jnp.float32).astype(
        jnp.bfloat16
    )
    arrived = lax.all_to_all(
        buffer.reshape(shards, per_device * capacity, local_width),
        "fs",
        split_axis=0,
        concat_axis=0,
        tiled=True,
    )
    arrived = arrived.reshape(shards, per_device, capacity, local_width)
    partial_value = lax.all_gather(arrived, "tp", axis=3, tiled=True)
    gate_sum = jnp.einsum(
        "sxcd,xdf->xscf", partial_value, gate_serve, preferred_element_type=jnp.float32
    )
    up_sum = jnp.einsum(
        "sxcd,xdf->xscf", partial_value, up_serve, preferred_element_type=jnp.float32
    )
    hidden = (jax.nn.silu(gate_sum) * up_sum).astype(jnp.bfloat16)
    products = jnp.einsum("xdf,xscf->dsxc", down_serve, hidden, preferred_element_type=jnp.float32)
    summed = lax.psum_scatter(
        products.reshape(local_width * lax.axis_size("tp"), shards * per_device * capacity).astype(
            jnp.bfloat16
        ),
        "tp",
        scatter_dimension=0,
        tiled=True,
    )
    returned = lax.all_to_all(
        summed.reshape(local_width, shards, per_device * capacity),
        "fs",
        split_axis=1,
        concat_axis=1,
        tiled=True,
    )
    returned = returned.reshape(local_width, experts * capacity)
    combined = jnp.zeros((tok_rows, local_width), jnp.float32)
    for rank_slot in range(top_count):
        picked = jnp.einsum(
            "ts,ds->td", selects[rank_slot], returned, preferred_element_type=jnp.float32
        )
        combined = combined + route_weights[:, rank_slot : rank_slot + 1] * picked
    return (gate_serve, up_serve, down_serve, combined.astype(jnp.bfloat16))


MESH = pl.DeviceIdType.MESH
bf16, f32, i32 = jnp.bfloat16, jnp.float32, jnp.int32


def remote(src, dst, send, recv, to):
    return pltpu.make_async_remote_copy(
        src_ref=src, dst_ref=dst, send_sem=send, recv_sem=recv, device_id=to, device_id_type=MESH
    )


def kernel(
    NF, NT, C,
    tokens, ids_t, weights_t, gain, gm, um, dm,
    gate_o, up_o, down_o, moe_o,
    gmv, umv, dmv, gcol, toks, ids_all, xg, invs, acc, comb, sd, sgu, wd, wgu, wdq, hid, rs, ret,
    ld_sem, i_send, i_recv, c_send, c_recv, p_sib, p_x, p_recv,
    wd_send, wd_recv, wdy_send, wdy_recv, gu_send, gu_recv, guy_send, guy_recv,
    wq_send, wq_recv, wq_own, h_sib, h_x, h_recv, r_send, r_recv, o_sem,
):
    g, f, t = lax.axis_index("grp"), lax.axis_index("fs"), lax.axis_index("tp")
    NX = NT // 2
    chip, core = t // 2, lax.rem(t, 2)
    sib = chip * 2 + (1 - core)
    H, Fl = dmv.shape[1], dmv.shape[2]
    Dl = 2 * H
    T, Dq = tokens.shape
    D = NT * Dq
    ring = range(1, NF)

    def fs_at(k):
        return lax.rem(f + k + NF, NF)

    def rows(s, half):
        return pl.ds(pl.multiple_of(s * Dl + half * H, H), H)

    def both(s):
        return pl.ds(pl.multiple_of(s * Dl, Dl), Dl)

    halves = [(fs_at(k), g) for k in range(NF)] + [(f, 1 - g)]
    order = list(ring) + [0, NF]
    loads = {}
    for m, src, dst in ((0, gm, gmv), (1, um, umv), (2, dm, dmv)):
        for k in order:
            e, half = halves[k]
            cp = pltpu.make_async_copy(
                src.at[e, pl.ds(pl.multiple_of(half * H, H), H), :], dst.at[k], ld_sem.at[m, k]
            )
            cp.start()
            loads[m, k] = cp

    barrier = pltpu.get_barrier_semaphore()
    for k in ring:
        pl.semaphore_signal(barrier, inc=1, device_id={"fs": fs_at(k)}, device_id_type=MESH)
    for k in range(1, NT):
        pl.semaphore_signal(barrier, inc=1, device_id={"tp": lax.rem(t + k, NT)}, device_id_type=MESH)
    peer = {"grp": 1 - g}
    pl.semaphore_signal(barrier, inc=1, device_id=peer, device_id_type=MESH)

    earlier = (
        lax.broadcasted_iota(i32, (T, T), 0) < lax.broadcasted_iota(i32, (T, T), 1)
    ).astype(bf16)
    c_iota = lax.broadcasted_iota(i32, (C, T), 0).astype(f32)

    def slot_row(ids, e):
        member = jnp.max((ids == e).astype(f32), axis=0, keepdims=True)
        pos = jnp.dot(
            jnp.broadcast_to(member, (8, T)).astype(bf16), earlier, preferred_element_type=f32
        )
        return jnp.where(member > 0, pos[:1], -1.0)

    def place(s, ids, block):
        hot = (c_iota == slot_row(ids, f)).astype(bf16)
        xg[t, s] = jnp.dot(hot, block[...], preferred_element_type=f32).astype(bf16)

    pl.semaphore_wait(barrier, (NF - 1) + (NT - 1) + 1)

    waits = []

    def go(cp):
        cp.start()
        waits.append(cp)

    for k in ring:
        go(remote(ids_t, ids_all.at[f], i_send.at[k], i_recv.at[f], {"fs": fs_at(k)}))

    parts = 2 if T % 32 == 0 else 1
    Tp = T // parts

    def hop(src, b, p, way):
        cut = pl.ds(p * Tp, Tp)
        return remote(
            src.at[cut, :], toks.at[b, cut, :], c_send.at[(1 - way) // 2, b, p], c_recv.at[b, p], {"fs": f + way}
        )

    @pl.when(f < NF - 1)
    def _():
        for p in range(parts):
            hop(tokens, f, p, 1).start()

    @pl.when(f > 0)
    def _():
        for p in range(parts):
            hop(tokens, f, p, -1).start()

    def spread(buf, sems_sib, sems_x, sems_recv, s):
        for dx in range(1, NX):
            other = lax.rem(chip + dx, NX)
            remote(
                buf.at[t, s], buf.at[t, s], sems_x.at[dx, s], sems_recv.at[t, s],
                {"tp": other * 2 + core},
            ).start()
        remote(buf.at[t, s], buf.at[t, s], sems_sib.at[t, s], sems_recv.at[t, s], {"tp": sib}).start()

    def arrived(buf, sems_recv, q, s):
        remote(buf.at[q, s], buf.at[q, s], sems_recv.at[q, s], sems_recv.at[q, s], {"tp": sib}).wait_recv()

    def pass_on(buf, sems_sib, sems_recv, s):
        for dx in range(1, NX):
            q = lax.rem(chip + dx, NX) * 2 + core
            arrived(buf, sems_recv, q, s)
            remote(buf.at[q, s], buf.at[q, s], sems_sib.at[q, s], sems_recv.at[q, s], {"tp": sib}).start()

    def sib_arrived(buf, sems_recv, s):
        for dx in range(NX):
            arrived(buf, sems_recv, lax.rem(chip + dx, NX) * 2 + 1 - core, s)

    def spread_sent(buf, sems_sib, sems_x, s):
        for dx in range(1, NX):
            remote(buf.at[t, s], buf.at[t, s], sems_x.at[dx, s], sems_x.at[dx, s], {"tp": sib}).wait_send()
        for dx in range(NX):
            q = lax.rem(chip + dx, NX) * 2 + core
            remote(buf.at[q, s], buf.at[q, s], sems_sib.at[q, s], sems_sib.at[q, s], {"tp": sib}).wait_send()

    place(f, ids_t[...], tokens)
    spread(xg, p_sib, p_x, p_recv, f)

    gcol[...] = jnp.transpose(jnp.broadcast_to(gain[...], (Fl, Dl)))
    mine = pl.ds(pl.multiple_of(g * H, H), H)
    theirs = pl.ds(pl.multiple_of((1 - g) * H, H), H)
    for k in ring:
        loads[0, k].wait()
        loads[1, k].wait()
        sgu[k, :, :Fl] = (gmv[k] * gcol[mine, :]).astype(bf16)
        sgu[k, :, Fl:] = (umv[k] * gcol[mine, :]).astype(bf16)
    for k in ring:
        loads[2, k].wait()
        sd[k] = dmv[k].astype(bf16)

    def gu_copy(k, e):
        return remote(sgu.at[k], wgu.at[rows(f, g), :], gu_send.at[k], gu_recv.at[f], {"fs": e})

    def wd_copy(k, e):
        return remote(sd.at[k], wd.at[rows(f, g), :], wd_send.at[k], wd_recv.at[f], {"fs": e})

    def send_weights(at, way):
        reach = NF - 1 - at if way > 0 else at
        for make in (gu_copy, wd_copy):
            for dist in range(1, reach + 1):
                make(way * dist % NF, at + way * dist).start()

    for k, half, part in ((0, g, mine), (NF, 1 - g, theirs)):
        for m in range(3):
            loads[m, k].wait()
        wd[rows(f, half), :] = dmv[k].astype(bf16)
        wgu[rows(f, half), :Fl] = (gmv[k] * gcol[part, :]).astype(bf16)
        wgu[rows(f, half), Fl:] = (umv[k] * gcol[part, :]).astype(bf16)

    for k in ring:
        s = fs_at(k)
        remote(ids_t, ids_all.at[s], i_recv.at[s], i_recv.at[s], {"fs": s}).wait_recv()

    def take(b):
        place(b, ids_all[b], toks.at[b])
        spread(xg, p_sib, p_x, p_recv, b)

    for d in ring:
        for p in range(parts):
            @pl.when(f >= d)
            def _():
                hop(tokens, f - d, p, 1).wait_recv()

                @pl.when(f < NF - 1)
                def _():
                    hop(toks.at[f - d], f - d, p, 1).start()

            @pl.when(f + d < NF)
            def _():
                hop(tokens, f + d, p, -1).wait_recv()

                @pl.when(f > 0)
                def _():
                    hop(toks.at[f + d], f + d, p, -1).start()

        for at in range(NF):
            if max(at, NF - 1 - at) == d:
                @pl.when(f == at)
                def _():
                    send_weights(at, 1)
                    send_weights(at, -1)

        @pl.when(f >= d)
        def _():
            take(f - d)

        @pl.when(f + d < NF)
        def _():
            take(f + d)

        if d == 1:
            pass_on(xg, p_sib, p_recv, f)
        else:
            @pl.when(f >= d - 1)
            def _():
                pass_on(xg, p_sib, p_recv, f - d + 1)

            @pl.when(f + d - 1 < NF)
            def _():
                pass_on(xg, p_sib, p_recv, f + d - 1)

    by_distance = [sorted((s for s in range(NF) if s != a), key=lambda s: abs(s - a)) for a in range(NF)]

    def pick(column):
        out = jnp.int32(column[0])
        for a in range(1, NF):
            out = jnp.where(f == a, jnp.int32(column[a]), out)
        return out

    near = [pick([by_distance[a][i] for a in range(NF)]) for i in range(NF - 1)]

    def to_peer(buf, y_send, y_recv, recv, s):
        here = buf.at[rows(s, g), :]
        remote(here, here, recv.at[s], recv.at[s], {"fs": s}).wait_recv()
        remote(here, here, y_send.at[s], y_recv.at[s], peer).start()

    def from_peer(buf, y_recv, s):
        there = buf.at[rows(s, 1 - g), :]
        remote(there, there, y_recv.at[s], y_recv.at[s], peer).wait_recv()

    to_peer(wgu, guy_send, guy_recv, gu_recv, near[0])
    for d in (NF - 1,):
        @pl.when(f >= d)
        def _():
            pass_on(xg, p_sib, p_recv, f - d)

        @pl.when(f + d < NF)
        def _():
            pass_on(xg, p_sib, p_recv, f + d)
    for s in near[1:]:
        to_peer(wgu, guy_send, guy_recv, gu_recv, s)

    for e in range(NF):
        w_row = jnp.sum(jnp.where(ids_t[...] == e, weights_t[...], 0.0), axis=0, keepdims=True)
        w_at = jnp.where(c_iota == slot_row(ids_t[...], e), w_row, 0.0)
        high = w_at.astype(bf16)
        comb[e, 0] = high
        comb[e, 1] = (w_at - high.astype(f32)).astype(bf16)

    for k in range(NF):
        s = fs_at(k)
        sib_arrived(xg, p_recv, s)
        sq = jnp.zeros((C, 1), f32)
        for q in range(NT):
            xf = xg[q, s].astype(f32)
            sq = sq + jnp.sum(xf * xf, axis=1, keepdims=True)
        invs[s] = jnp.broadcast_to(lax.rsqrt(sq / D + norm_epsilon), (C, Fl))

    def partial_sums(q, first):
        w = wgu[both(q), :]
        for s in range(NF):
            part = jnp.dot(xg[q, s], w, preferred_element_type=f32)
            acc[s] = part if first else acc[s] + part

    def turned(s, half):
        part = pl.ds(pl.multiple_of(half * H, H), H)
        return remote(
            wd.at[rows(s, half), :], wdq.at[t, part, :], wq_send.at[s, half], wq_recv.at[t, half], {"tp": s}
        )

    own_q = pltpu.make_async_copy(wd.at[both(t), :], wdq.at[t], wq_own)

    def turn(s, half):
        @pl.when(s != t)
        def _():
            turned(s, half).start()

    turn(f, 0)
    turn(f, 1)
    partial_sums(f, True)
    for s in near:
        from_peer(wgu, guy_recv, s)
        partial_sums(s, False)
        to_peer(wd, wdy_send, wdy_recv, wd_recv, s)
        turn(s, g)
    outs = [
        pltpu.make_async_copy(wgu.at[:, :Fl], gate_o.at[0], o_sem.at[0]),
        pltpu.make_async_copy(wgu.at[:, Fl:], up_o.at[0], o_sem.at[1]),
        pltpu.make_async_copy(wd, down_o.at[0], o_sem.at[2]),
    ]
    outs[0].start()
    outs[1].start()

    far = near[::-1] + [f]
    for s in far:
        sums = acc[s]
        gate, up = sums[:, :Fl] * invs[s], sums[:, Fl:] * invs[s]
        hid[t, s] = (gate / (1.0 + jnp.exp(-gate)) * up).astype(bf16)
        spread(hid, h_sib, h_x, h_recv, s)

    for s in near:
        from_peer(wd, wdy_recv, s)
        turn(s, 1 - g)
    own_q.start()
    outs[2].start()
    for s in far:
        pass_on(hid, h_sib, h_recv, s)
    own_q.wait()
    for k in range(1, NT):
        q = lax.rem(t + k, NT)
        for half in range(2):
            part = wdq.at[q, half * H : (half + 1) * H, :]
            remote(part, part, wq_recv.at[q, half], wq_recv.at[q, half], {"tp": q}).wait_recv()
    for i, s in enumerate(far):
        sib_arrived(hid, h_recv, s)
        h = jnp.concatenate([hid[q, s] for q in range(NT)], axis=1)
        w = jnp.concatenate([wdq[q] for q in range(NT)], axis=1)
        y = lax.dot_general(h, w, (((1,), (1,)), ((), ())), preferred_element_type=f32).astype(bf16)
        if i == NF - 1:
            ret[f] = y
        else:
            rs[s] = y
            go(remote(rs.at[s], ret.at[f], r_send.at[s], r_recv.at[f], {"fs": s}))

    total = jnp.zeros((T, Dq), f32)
    for i, e in enumerate([f] + near):
        if i:
            remote(rs.at[e], ret.at[e], r_recv.at[e], r_recv.at[e], {"fs": e}).wait_recv()
        for term in range(2):
            total = total + lax.dot_general(
                comb[e, term], ret[e], (((0,), (0,)), ((), ())), preferred_element_type=f32
            )
    moe_o[...] = total.astype(bf16)

    for cp in outs:
        cp.wait()
    for cp in waits:
        cp.wait_send()
    for k in ring:
        s = fs_at(k)
        gu_copy(k, s).wait_send()
        wd_copy(k, s).wait_send()
        for buf, y_send in ((wgu, guy_send), (wd, wdy_send)):
            here = buf.at[rows(s, g), :]
            remote(here, here, y_send.at[s], y_send.at[s], peer).wait_send()
    for s in range(NF):
        @pl.when(s != t)
        def _():
            turned(s, 0).wait_send()
            turned(s, 1).wait_send()

        spread_sent(xg, p_sib, p_x, s)
        spread_sent(hid, h_sib, h_x, s)

        for p in range(parts):
            @pl.when((s <= f) & (f < NF - 1))
            def _():
                hop(tokens, s, p, 1).wait_send()

            @pl.when((s >= f) & (f > 0))
            def _():
                hop(tokens, s, p, -1).wait_send()


def finish(n, pieces, *refs):
    ins, outs, stage, sems = refs[:n], refs[n : 2 * n], refs[2 * n : 3 * n], refs[3 * n]
    cuts = []
    for i, ref in enumerate(ins):
        size = ref.shape[-2] // pieces
        for p in range(pieces):
            at = (0,) * (len(ref.shape) - 2) + (pl.ds(p * size, size), slice(None))
            cuts.append((i, p, at))
    there = {}
    for i, p, at in cuts:
        there[i, p] = pltpu.make_async_copy(ins[i].at[at], stage[i].at[at], sems.at[0, i, p])
        there[i, p].start()
    back = []
    for i, p, at in cuts:
        there[i, p].wait()
        cp = pltpu.make_async_copy(stage[i].at[at], outs[i].at[at], sems.at[1, i, p])
        cp.start()
        back.append(cp)
    for cp in back:
        cp.wait()


def fused(tokens, route_ids, route_weights, norm_gain, gate_master, up_master, down_master):
    NF, NT = lax.axis_size("fs"), lax.axis_size("tp")
    E, Dl, Fl = gate_master.shape
    T, Dq = tokens.shape
    K = route_ids.shape[1]
    capacity = max(2, 3 * T * K // (2 * E))
    C = -(-capacity // 8) * 8
    H = Dl // 2
    D = Dl * NF
    NX = NT // 2
    dma = pltpu.SemaphoreType.DMA
    vmem, hbm = pl.BlockSpec(memory_space=pltpu.VMEM), pl.BlockSpec(memory_space=pl.ANY)
    serve = jax.ShapeDtypeStruct((1, D, Fl), bf16)
    done = pl.pallas_call(
        functools.partial(kernel, NF, NT, C),
        out_shape=(serve, serve, serve, jax.ShapeDtypeStruct((T, Dq), bf16)),
        in_specs=[vmem] * 4 + [hbm] * 3,
        out_specs=(hbm, hbm, hbm, vmem),
        scratch_shapes=[
            pltpu.VMEM((NF + 1, H, Fl), f32),
            pltpu.VMEM((NF + 1, H, Fl), f32),
            pltpu.VMEM((NF + 1, H, Fl), f32),
            pltpu.VMEM((Dl, Fl), f32),
            pltpu.VMEM((NF, T, Dq), bf16),
            pltpu.VMEM((NF, K, T), i32),
            pltpu.VMEM((NT, NF, C, Dq), bf16),
            pltpu.VMEM((NF, C, Fl), f32),
            pltpu.VMEM((NF, C, 2 * Fl), f32),
            pltpu.VMEM((NF, 2, C, T), bf16),
            pltpu.VMEM((NF, H, Fl), bf16),
            pltpu.VMEM((NF, H, 2 * Fl), bf16),
            pltpu.VMEM((D, Fl), bf16),
            pltpu.VMEM((D, 2 * Fl), bf16),
            pltpu.VMEM((NT, Dq, Fl), bf16),
            pltpu.VMEM((NT, NF, C, Fl), bf16),
            pltpu.VMEM((NF, C, Dq), bf16),
            pltpu.VMEM((NF, C, Dq), bf16),
            dma((3, NF + 1)),
            dma((NF,)), dma((NF,)),
            dma((2, NF, 2)), dma((NF, 2)),
            dma((NT, NF)), dma((NX, NF)), dma((NT, NF)),
            dma((NF,)), dma((NF,)), dma((NF,)), dma((NF,)),
            dma((NF,)), dma((NF,)), dma((NF,)), dma((NF,)),
            dma((NT, 2)), dma((NT, 2)), dma(()),
            dma((NT, NF)), dma((NX, NF)), dma((NT, NF)),
            dma((NF,)), dma((NF,)),
            dma((3,)),
        ],
        compiler_params=pltpu.CompilerParams(
            collective_id=0, has_side_effects=True, vmem_limit_bytes=56 * 1024 * 1024
        ),
    )(
        tokens, route_ids.T, route_weights.T, norm_gain[None, :],
        gate_master, up_master, down_master,
    )
    pieces = 2 if T % 32 == 0 else 1
    return pl.pallas_call(
        functools.partial(finish, len(done), pieces),
        out_shape=tuple(jax.ShapeDtypeStruct(a.shape, a.dtype) for a in done),
        in_specs=[hbm] * len(done),
        out_specs=(hbm,) * len(done),
        scratch_shapes=[pltpu.VMEM(a.shape, a.dtype) for a in done] + [dma((2, len(done), pieces))],
        compiler_params=pltpu.CompilerParams(vmem_limit_bytes=56 * 1024 * 1024),
    )(*done)


def solution(mesh):
    shape = mesh.shape
    fits = shape['grp'] == 2 and shape['tp'] % 2 == 0 and shape['fs'] == shape['tp'] <= 8
    body = fused if fits else local
    placed = (
        P(("grp", "fs"), "tp"),
        P(("grp", "fs"), None),
        P(("grp", "fs"), None),
        P("fs"),
        P(None, "fs", "tp"),
        P(None, "fs", "tp"),
        P(None, "fs", "tp"),
    )
    return jax.shard_map(
        body,
        mesh=mesh,
        in_specs=placed,
        out_specs=(
            P(("grp", "fs"), None, "tp"),
            P(("grp", "fs"), None, "tp"),
            P(("grp", "fs"), None, "tp"),
            P(("grp", "fs"), "tp"),
        ),
        check_vma=False,
    )
```

profile of v0, /device:TPU:0, one launch (start us, length us, event | category | flops | bytes accessed | tf_op | source)
XLA Modules:
  0.0 65.5 jit_solution(6893871566327364936)
XLA Ops:
  0.6 62.6 %shard_map.102 = (bf16[1,2048,128]{2,1,0:T(8,128)(2,1)}, bf16[1,2048,128]{2,1,0:T(8,128)(2,1)}, bf16[1,2048,128]{2,1,0:T(8,128)(2,1)}, bf16[224,512]{1,0:T(8,128)(2,1)}) custom-call(bf16[224,512]{1,0:T(8,128)(2,1)} %tokens.1, s32[2,224]{1,0:T(2,128)} %bitcast.3, f32[2,224]{1,0:T(2,128)} %bitcast.4, f32[1,512]{1,0:T(1,128)} %bitcast.5, f32[4,512,128]{2,1,0:T(8,128)} %gm.1, ...), custom_call_target="tpu_custom_call" | custom-call | tf_op jit(solution)/shard_map/pallas_call | solution.py:504
  63.2 2.3 %shard_map.103 = (bf16[1,2048,128]{2,1,0:T(8,128)(2,1)}, bf16[1,2048,128]{2,1,0:T(8,128)(2,1)}, bf16[1,2048,128]{2,1,0:T(8,128)(2,1)}, bf16[224,512]{1,0:T(8,128)(2,1)}) custom-call(bf16[1,2048,128]{2,1,0:T(8,128)(2,1)} %get-tuple-element.8.refs_0_, bf16[1,2048,128]{2,1,0:T(8,128)(2,1)} %get-tuple-element.9.refs_1_, ...), custom_call_target="tpu_custom_call" | custom-call | tf_op jit(solution)/shard_map/pallas_call | solution.py:547
where the time goes:
time: 66.2 us; the launch traced here: 65.5 us
  Pallas kernels  64.9 us (98%)
    pallas_call x1, Pallas kernels, fused(): pl.pallas_call(functools.partial(kernel, NF, NT, C), out_shape=(serve, se...  62.6 us
    pallas_call x1, Pallas kernels, fused(): pl.pallas_call(functools.partial(finish, len(done), pieces), out_shape=tu...  2.29 us

commit v1 on v0

v1 whole, which is shorter than its diff:
```python
import jax
import jax.numpy as jnp
from jax import lax
from jax.experimental import pallas as pl
from jax.experimental.pallas import tpu as pltpu
from jax.sharding import PartitionSpec as P

norm_epsilon = 1e-06


def slot_numbers(route_ids, experts, capacity):
    flat_ids = route_ids.reshape(-1)
    onehot = (flat_ids[:, None] == jnp.arange(experts, dtype=jnp.int32)[None, :]).astype(jnp.int32)
    before = jnp.cumsum(onehot, axis=0) - onehot
    position = jnp.sum(before * onehot, axis=1)
    return (flat_ids * capacity + position).reshape(route_ids.shape)


def local(tokens, route_ids, route_weights, norm_gain, gate_master, up_master, down_master):
    experts = gate_master.shape[0]
    shards = lax.axis_size("fs")
    columns = lax.axis_size("tp")
    per_device = experts // shards
    tok_rows = route_ids.shape[0]
    top_count = route_ids.shape[1]
    local_width = tokens.shape[1]
    model_width = local_width * columns
    capacity = max(2, 3 * tok_rows * top_count // (2 * experts))
    row_gain = norm_gain[None, :, None]
    gate_half = (gate_master * row_gain).astype(jnp.bfloat16)
    up_half = (up_master * row_gain).astype(jnp.bfloat16)
    down_half = down_master.astype(jnp.bfloat16)
    gate_serve, up_serve, down_serve = (
        lax.all_to_all(gate_half, "fs", split_axis=0, concat_axis=1, tiled=True),
        lax.all_to_all(up_half, "fs", split_axis=0, concat_axis=1, tiled=True),
        lax.all_to_all(down_half, "fs", split_axis=0, concat_axis=1, tiled=True),
    )
    slot_ids = slot_numbers(route_ids, experts, capacity)
    slot_range = jnp.arange(experts * capacity, dtype=jnp.int32)
    selects = [
        (slot_ids[:, rank_slot, None] == slot_range[None, :]).astype(jnp.bfloat16)
        for rank_slot in range(top_count)
    ]
    placing = selects[0]
    for extra in selects[1:]:
        placing = placing + extra
    local_values = tokens.astype(jnp.float32)
    squares = lax.psum(jnp.sum(local_values * local_values, axis=1), "tp")
    inverse = lax.rsqrt(squares / model_width + norm_epsilon)[:, None]
    normed = (local_values * inverse).astype(jnp.bfloat16)
    buffer = jnp.einsum("ts,td->sd", placing, normed, preferred_element_type=jnp.float32).astype(
        jnp.bfloat16
    )
    arrived = lax.all_to_all(
        buffer.reshape(shards, per_device * capacity, local_width),
        "fs",
        split_axis=0,
        concat_axis=0,
        tiled=True,
    )
    arrived = arrived.reshape(shards, per_device, capacity, local_width)
    partial_value = lax.all_gather(arrived, "tp", axis=3, tiled=True)
    gate_sum = jnp.einsum(
        "sxcd,xdf->xscf", partial_value, gate_serve, preferred_element_type=jnp.float32
    )
    up_sum = jnp.einsum(
        "sxcd,xdf->xscf", partial_value, up_serve, preferred_element_type=jnp.float32
    )
    hidden = (jax.nn.silu(gate_sum) * up_sum).astype(jnp.bfloat16)
    products = jnp.einsum("xdf,xscf->dsxc", down_serve, hidden, preferred_element_type=jnp.float32)
    summed = lax.psum_scatter(
        products.reshape(local_width * lax.axis_size("tp"), shards * per_device * capacity).astype(
            jnp.bfloat16
        ),
        "tp",
        scatter_dimension=0,
        tiled=True,
    )
    returned = lax.all_to_all(
        summed.reshape(local_width, shards, per_device * capacity),
        "fs",
        split_axis=1,
        concat_axis=1,
        tiled=True,
    )
    returned = returned.reshape(local_width, experts * capacity)
    combined = jnp.zeros((tok_rows, local_width), jnp.float32)
    for rank_slot in range(top_count):
        picked = jnp.einsum(
            "ts,ds->td", selects[rank_slot], returned, preferred_element_type=jnp.float32
        )
        combined = combined + route_weights[:, rank_slot : rank_slot + 1] * picked
    return (gate_serve, up_serve, down_serve, combined.astype(jnp.bfloat16))


MESH = pl.DeviceIdType.MESH
bf16, f32, i32 = jnp.bfloat16, jnp.float32, jnp.int32
GU_CUT, DN_CUT = 2, 4


def remote(src, dst, send, recv, to):
    return pltpu.make_async_remote_copy(
        src_ref=src, dst_ref=dst, send_sem=send, recv_sem=recv, device_id=to, device_id_type=MESH
    )


def kernel(
    tokens, ids_h, weights_h, gain_h, gm, um, dm,
    wgu, wd, moe,
    xt, ids, weights, gain, gcol, mv, sgu, sd, acc, inv, scale, wrow, wsend, hid,
    ss, sr, xs, xr, keep, zs, zr,
    in_sem, ld_sem, c_send, c_recv, w_send, w_recv, p_sib, p_x, p_recv,
    gu_send, gu_recv, guy_send, guy_recv, dn_send, dn_recv, dny_send, dny_recv,
    s_send, s_recv, x_send, x_recv, z_send, z_recv,
):
    g, f, t = lax.axis_index("grp"), lax.axis_index("fs"), lax.axis_index("tp")
    H, Fl = mv.shape[2:]
    Dl = 2 * H
    T, Dq = tokens.shape
    NT = xt.shape[0]
    D = NT * Dq
    Rg, Rd = H // GU_CUT, H // DN_CUT
    units = Dl // Fl
    per_half = units // 2
    pair, me = f // 2, lax.rem(f, 2)
    chip, core = t // 2, lax.rem(t, 2)
    mate = f + 1 - 2 * me
    twin = f + 2 - 4 * pair
    mate_twin = mate + 2 - 4 * pair
    far_a, far_b = 2 - pair, 3 - 3 * pair
    sib, over = {"tp": t + 1 - 2 * core}, {"tp": t + 2 - 4 * chip}
    peer, to_mate = {"grp": 1 - g}, {"fs": mate}
    mine_rows, mate_rows = (pl.ds(pl.multiple_of(i * T, T), T) for i in (me, 1 - me))
    inner = (f + 1) // 2 % 2 == 1
    home = chip == pair

    def cut(s, half, p, n):
        return pl.ds(pl.multiple_of(s * Dl + half * H + p * n, n), n)

    def both(s):
        return pl.ds(pl.multiple_of(s * Dl, Dl), Dl)

    small = [
        pltpu.make_async_copy(gain_h, gain, in_sem.at[0]),
        pltpu.make_async_copy(tokens, xt.at[t, mine_rows, :], in_sem.at[1]),
        pltpu.make_async_copy(ids_h, ids, in_sem.at[2]),
        pltpu.make_async_copy(weights_h, weights, in_sem.at[3]),
    ]
    small[0].start()
    small[1].start()
    picks = [
        (1 - me, g), (1 - me + 2, g), (me, g), (me + 2, g), (me, 1 - g), (me + 2, 1 - g),
    ]
    loads = {}
    for k, m in [(k, m) for k in (0, 2, 1, 3) for m in (0, 1)] + [
        (k, 2) for k in (0, 1, 2, 3)
    ] + [(k, m) for k in (4, 5) for m in (0, 1, 2)]:
        e, half = picks[k]
        loads[k, m] = pltpu.make_async_copy(
            (gm, um, dm)[m].at[e, pl.ds(pl.multiple_of(half * H, H), H), :],
            mv.at[m, k], ld_sem.at[m, k],
        )
        loads[k, m].start()
    small[2].start()
    small[3].start()

    barrier = pltpu.get_barrier_semaphore()
    friends = [to_mate, {"fs": twin}, {"fs": mate_twin}, peer, sib, over]
    for who in friends:
        pl.semaphore_signal(barrier, inc=1, device_id=who, device_id_type=MESH)

    small[0].wait()
    gcol[...] = jnp.transpose(jnp.broadcast_to(gain[...], (Fl, Dl)))
    mine_half = pl.ds(pl.multiple_of(g * H, H), H)
    other_half = pl.ds(pl.multiple_of((1 - g) * H, H), H)
    small[1].wait()
    pl.semaphore_wait(barrier, len(friends))

    def tok(q, rows):
        return xt.at[q, rows, :]

    token_hop = remote(tok(t, mine_rows), tok(t, mine_rows), c_send, c_recv, to_mate)
    token_hop.start()

    def spread(rows, i):
        block = tok(t, rows)
        remote(block, block, p_x.at[i], p_recv.at[t, i], over).start()
        remote(block, block, p_sib.at[t, i], p_recv.at[t, i], sib).start()

    def pass_on(rows, i):
        q = t + 2 - 4 * chip
        block = tok(q, rows)
        remote(block, block, p_recv.at[q, i], p_recv.at[q, i], sib).wait_recv()
        remote(block, block, p_sib.at[q, i], p_recv.at[q, i], sib).start()

    def sib_arrived(rows, i):
        for c in range(2):
            q = 2 * c + 1 - core
            block = tok(q, rows)
            remote(block, block, p_recv.at[q, i], p_recv.at[q, i], sib).wait_recv()

    spread(mine_rows, me)

    def gu_copy(kind, slot, p):
        src = (
            wgu.at[slot, cut(f, g, p, Rg), :] if kind == 0 else sgu.at[slot, p * Rg : (p + 1) * Rg, :]
        )
        return remote(
            src, wgu.at[slot, cut(f, g, p, Rg), :], gu_send.at[kind, slot, p],
            gu_recv.at[f, slot, p], {"fs": (twin, mate_twin, mate)[kind]},
        )

    def dn_copy(kind, p):
        src = wd.at[cut(f, g, p, Rd), :] if kind == 0 else sd.at[p * Rd : (p + 1) * Rd, :]
        return remote(
            src, wd.at[cut(f, g, p, Rd), :], dn_send.at[kind, p], dn_recv.at[f, p],
            {"fs": (twin, mate_twin, mate)[kind]},
        )

    def send_gu(slot, kinds):
        for p in range(GU_CUT):
            for kind in kinds:
                gu_copy(kind, slot, p).start()

    def send_dn(kinds):
        for p in range(DN_CUT):
            for kind in kinds:
                dn_copy(kind, p).start()

    def gu_ready(slot, k, dst, part):
        loads[k, 0].wait()
        loads[k, 1].wait()
        dst[:, :Fl] = (mv[0, k] * gcol[part, :]).astype(bf16)
        dst[:, Fl:] = (mv[1, k] * gcol[part, :]).astype(bf16)

    own_gu = [wgu.at[slot, cut(f, g, 0, H), :] for slot in range(2)]
    gu_ready(0, 0, sgu.at[0], mine_half)

    @pl.when(inner)
    def _():
        send_gu(0, (1, 2))

    @pl.when(jnp.logical_not(inner))
    def _():
        send_gu(0, (2,))

    gu_ready(0, 2, own_gu[0], mine_half)

    @pl.when(inner)
    def _():
        send_gu(0, (0,))

    gu_ready(1, 1, sgu.at[1], mine_half)

    @pl.when(inner)
    def _():
        send_gu(1, (1, 2))

    @pl.when(jnp.logical_not(inner))
    def _():
        send_gu(1, (2,))

    gu_ready(1, 3, own_gu[1], mine_half)

    @pl.when(inner)
    def _():
        send_gu(1, (0,))

    @pl.when(jnp.logical_not(inner))
    def _():
        send_gu(0, (0, 1))
        send_gu(1, (0, 1))

    for k in range(4):
        loads[k, 2].wait()
    for slot in range(2):
        lanes = slice(slot * Fl, (slot + 1) * Fl)
        sd[:, lanes] = mv[2, slot].astype(bf16)
        wd[cut(f, g, 0, H), lanes] = mv[2, 2 + slot].astype(bf16)
    send_dn((2,))

    @pl.when(jnp.logical_not(inner))
    def _():
        send_dn((0, 1))

    for slot in range(2):
        lanes = slice(slot * Fl, (slot + 1) * Fl)
        gu_ready(slot, 4 + slot, wgu.at[slot, cut(f, 1 - g, 0, H), :], other_half)
        loads[4 + slot, 2].wait()
        wd[cut(f, 1 - g, 0, H), lanes] = mv[2, 4 + slot].astype(bf16)

    small[2].wait()
    small[3].wait()
    wrow[me] = jnp.zeros(wsend.shape, f32)
    wsend[...] = jnp.zeros(wsend.shape, f32)
    for slot in range(2):
        for ref, parity in ((wrow.at[me], me), (wsend, 1 - me)):
            row = jnp.where(ids[...] == parity + 2 * slot, weights[...], 0.0)
            ref[slot : slot + 1, :T] = jnp.sum(row, axis=0, keepdims=True)
    w_hop = remote(wsend, wrow.at[me], w_send, w_recv, to_mate)
    w_hop.start()

    remote(tok(t, mate_rows), tok(t, mate_rows), c_send, c_recv, to_mate).wait_recv()
    spread(mate_rows, 1 - me)

    def gu_forward(s, slot, p):
        here = wgu.at[slot, cut(s, g, p, Rg), :]
        remote(here, here, gu_recv.at[s, slot, p], gu_recv.at[s, slot, p], peer).wait_recv()
        remote(here, here, guy_send.at[s, slot, p], guy_recv.at[s, slot, p], peer).start()

    def gu_peer(s, slot):
        for p in range(GU_CUT):
            there = wgu.at[slot, cut(s, 1 - g, p, Rg), :]
            remote(there, there, guy_recv.at[s, slot, p], guy_recv.at[s, slot, p], peer).wait_recv()

    def dn_forward(s, p):
        here = wd.at[cut(s, g, p, Rd), :]
        remote(here, here, dn_recv.at[s, p], dn_recv.at[s, p], peer).wait_recv()
        remote(here, here, dny_send.at[s, p], dny_recv.at[s, p], peer).start()

    def dn_peer(s, p):
        there = wd.at[cut(s, 1 - g, p, Rd), :]
        remote(there, there, dny_recv.at[s, p], dny_recv.at[s, p], peer).wait_recv()

    def gu_all(s, slot):
        for p in range(GU_CUT):
            gu_forward(s, slot, p)

    def partial_sums(s, slot):
        return jnp.dot(xt[s], wgu[slot, both(s), :], preferred_element_type=f32)

    gu_all(mate, 0)
    gu_all(far_a, 0)
    pass_on(mine_rows, me)
    gu_all(mate, 1)
    gu_all(far_a, 1)
    pass_on(mate_rows, 1 - me)

    remote(wsend, wrow.at[1 - me], w_recv, w_recv, to_mate).wait_recv()
    sib_arrived(mine_rows, me)
    sib_arrived(mate_rows, 1 - me)
    for i in range(2):
        rows = slice(i * T, (i + 1) * T)
        sq = jnp.zeros((T, Fl), f32)
        for q in range(NT):
            for c in range(Dq // Fl):
                part = xt[q, rows, c * Fl : (c + 1) * Fl].astype(f32)
                sq = sq + part * part
        root = lax.rsqrt(jnp.sum(sq, axis=1, keepdims=True) / D + norm_epsilon)
        inv[rows, :] = jnp.broadcast_to(root, (T, Fl))
        for slot in range(2):
            wide = jnp.transpose(
                jnp.broadcast_to(wrow[i, slot : slot + 1, :], (Fl, wrow.shape[2]))
            )
            scale[slot, rows, :] = wide[:T] * root

    for slot in range(2):
        acc[slot] = partial_sums(f, slot)
    for slot in range(2):
        for s in (mate, far_a):
            gu_peer(s, slot)
            acc[slot] += partial_sums(s, slot)

    gu_all(far_b, 0)
    gu_forward(far_b, 1, 0)

    @pl.when(inner)
    def _():
        send_dn((0, 1))

    for p in range(1, GU_CUT):
        gu_forward(far_b, 1, p)
    for p in range(DN_CUT):
        dn_forward(mate, p)

    for slot in range(2):
        gu_peer(far_b, slot)
        sums = acc[slot] + partial_sums(far_b, slot)
        gate, up = sums[:, :Fl] * inv[...], sums[:, Fl:] * scale[slot]
        hid[:, slot * Fl : (slot + 1) * Fl] = (gate / (1.0 + jnp.exp(-gate)) * up).astype(bf16)

    near_mine, near_theirs = 2 * pair + core, 2 * pair + 1 - core
    far_mine, far_theirs = 2 - 2 * pair + core, 2 - 2 * pair + 1 - core

    def out_part(s, u, n):
        rows = pl.ds(pl.multiple_of(s * Dl + u * Fl, Fl), n * Fl)
        return lax.dot_general(
            hid[...], wd[rows, :], (((1,), (1,)), ((), ())), preferred_element_type=f32
        )

    def swap(n, u, count):
        at = pl.ds(u, count)
        return remote(ss.at[n, at], sr.at[n, at], s_send.at[n, u], s_recv.at[n, u], sib)

    def cross(u, count):
        at = pl.ds(u, count)
        return remote(xs.at[at], xr.at[at], x_send.at[u], x_recv.at[u], over)

    def back(u, count):
        at = pl.ds(u, count)
        return remote(zs.at[at], zr.at[at], z_send.at[u], z_recv.at[u], to_mate)

    def theirs(n, s, u, count):
        y = out_part(s, u, count)
        for j in range(count):
            ss[n, u + j] = y[:, j * Fl : (j + 1) * Fl].astype(bf16)
        swap(n, u, count).start()

    def mine(n, s, u, count):
        y = out_part(s, u, count)
        swap(n, u, count).wait_recv()
        kept = home if n == 0 else jnp.logical_not(home)
        parts = [y[:, j * Fl : (j + 1) * Fl] + sr[n, u + j].astype(f32) for j in range(count)]

        @pl.when(kept)
        def _():
            for j in range(count):
                keep[u + j] = parts[j]

        @pl.when(jnp.logical_not(kept))
        def _():
            for j in range(count):
                xs[u + j] = parts[j].astype(bf16)
            cross(u, count).start()

    def give_back(u, count):
        cross(u, count).wait_recv()
        for j in range(count):
            zs[u + j] = (keep[u + j, mate_rows, :] + xr[u + j, mate_rows, :].astype(f32)).astype(bf16)
        back(u, count).start()

    def finish(u, count):
        back(u, count).wait_recv()
        for j in range(count):
            lane = (u + j) * Fl
            lanes = pl.ds(lane if isinstance(lane, int) else pl.multiple_of(lane, Fl), Fl)
            moe[:, lanes] = (
                keep[u + j, mine_rows, :] + xr[u + j, mine_rows, :].astype(f32) + zr[u + j].astype(f32)
            ).astype(bf16)

    ratio = DN_CUT // per_half

    def far_forward(j):
        for p in range(j * ratio, (j + 1) * ratio):
            dn_forward(far_a, p)
            dn_forward(far_b, p)

    def far_peer(j):
        for p in range(j * ratio, (j + 1) * ratio):
            dn_peer(far_a, p)
            dn_peer(far_b, p)

    for p in range(DN_CUT):
        dn_peer(mate, p)
    for h in range(2):
        theirs(0, near_theirs, h * per_half, per_half)
    for h in range(2):
        mine(0, near_mine, h * per_half, per_half)

    for j in range(per_half):
        far_forward(j)
        for half in (g, 1 - g):
            u = half * per_half + j
            if half is not g:
                far_peer(j)
            theirs(1, far_theirs, u, 1)
            mine(1, far_mine, u, 1)
        if j == 0:
            @pl.when(home)
            def _():
                for h in range(2):
                    give_back(h * per_half, per_half)

    @pl.when(home)
    def _():
        for h in range(2):
            finish(h * per_half, per_half)

    @pl.when(jnp.logical_not(home))
    def _():
        order = [half * per_half + j for j in range(per_half) for half in (g, 1 - g)]
        for u in order:
            give_back(u, 1)
        for u in order:
            finish(u, 1)

    token_hop.wait_send()
    w_hop.wait_send()
    for i, rows in ((me, mine_rows), (1 - me, mate_rows)):
        block = tok(t, rows)
        remote(block, block, p_x.at[i], p_x.at[i], over).wait_send()
        for q in (t, t + 2 - 4 * chip):
            remote(block, block, p_sib.at[q, i], p_sib.at[q, i], sib).wait_send()
    for kind in range(3):
        for slot in range(2):
            for p in range(GU_CUT):
                gu_copy(kind, slot, p).wait_send()
        for p in range(DN_CUT):
            dn_copy(kind, p).wait_send()
    for s in (mate, far_a, far_b):
        for slot in range(2):
            for p in range(GU_CUT):
                here = wgu.at[slot, cut(s, g, p, Rg), :]
                remote(here, here, guy_send.at[s, slot, p], guy_send.at[s, slot, p], peer).wait_send()
        for p in range(DN_CUT):
            here = wd.at[cut(s, g, p, Rd), :]
            remote(here, here, dny_send.at[s, p], dny_send.at[s, p], peer).wait_send()
    for h in range(2):
        swap(0, h * per_half, per_half).wait_send()
    for u in range(units):
        swap(1, u, 1).wait_send()

    @pl.when(home)
    def _():
        for u in range(units):
            cross(u, 1).wait_send()
        for h in range(2):
            back(h * per_half, per_half).wait_send()

    @pl.when(jnp.logical_not(home))
    def _():
        for h in range(2):
            cross(h * per_half, per_half).wait_send()
        for u in range(units):
            back(u, 1).wait_send()


def finish_kernel(wgu, wd, moe, gate_o, up_o, down_o, moe_o, sems):
    Fl = gate_o.shape[2]
    slot = lax.axis_index("fs") // 2
    lanes = pl.ds(pl.multiple_of(slot * Fl, Fl), Fl)
    copies = [
        pltpu.make_async_copy(wgu.at[slot, :, :Fl], gate_o.at[0], sems.at[0]),
        pltpu.make_async_copy(wgu.at[slot, :, Fl:], up_o.at[0], sems.at[1]),
        pltpu.make_async_copy(wd.at[:, lanes], down_o.at[0], sems.at[2]),
        pltpu.make_async_copy(moe, moe_o, sems.at[3]),
    ]
    for cp in copies:
        cp.start()
    for cp in copies:
        cp.wait()


def fused(tokens, route_ids, route_weights, norm_gain, gate_master, up_master, down_master):
    NF, NT = lax.axis_size("fs"), lax.axis_size("tp")
    E, Dl, Fl = gate_master.shape
    T, Dq = tokens.shape
    K = route_ids.shape[1]
    H = Dl // 2
    D = Dl * NF
    Tw = -(-T // 128) * 128
    units = Dl // Fl
    dma = pltpu.SemaphoreType.DMA
    vmem, hbm = pl.BlockSpec(memory_space=pltpu.VMEM), pl.BlockSpec(memory_space=pl.ANY)
    gu, dn = (NF, 2, GU_CUT), (NF, DN_CUT)
    ins = (
        tokens, route_ids.T, route_weights.T, norm_gain[None, :],
        gate_master, up_master, down_master,
    )
    done = pl.pallas_call(
        kernel,
        out_shape=(
            pltpu.VMEM((2, D, 2 * Fl), bf16), pltpu.VMEM((D, 2 * Fl), bf16), pltpu.VMEM((T, Dq), bf16),
        ),
        in_specs=[hbm] * 7,
        out_specs=(vmem,) * 3,
        scratch_shapes=[
            pltpu.VMEM((NT, 2 * T, Dq), bf16),
            pltpu.VMEM((K, T), i32),
            pltpu.VMEM((K, T), f32),
            pltpu.VMEM((1, Dl), f32),
            pltpu.VMEM((Dl, Fl), f32),
            pltpu.VMEM((3, 6, H, Fl), f32),
            pltpu.VMEM((2, H, 2 * Fl), bf16),
            pltpu.VMEM((H, 2 * Fl), bf16),
            pltpu.VMEM((2, 2 * T, 2 * Fl), f32),
            pltpu.VMEM((2 * T, Fl), f32),
            pltpu.VMEM((2, 2 * T, Fl), f32),
            pltpu.VMEM((2, 8, Tw), f32),
            pltpu.VMEM((8, Tw), f32),
            pltpu.VMEM((2 * T, 2 * Fl), bf16),
            pltpu.VMEM((2, units, 2 * T, Fl), bf16),
            pltpu.VMEM((2, units, 2 * T, Fl), bf16),
            pltpu.VMEM((units, 2 * T, Fl), bf16),
            pltpu.VMEM((units, 2 * T, Fl), bf16),
            pltpu.VMEM((units, 2 * T, Fl), f32),
            pltpu.VMEM((units, T, Fl), bf16),
            pltpu.VMEM((units, T, Fl), bf16),
            dma((4,)), dma((3, 6)),
            dma(()), dma(()), dma(()), dma(()),
            dma((NT, 2)), dma((2,)), dma((NT, 2)),
            dma((3, 2, GU_CUT)), dma(gu), dma(gu), dma(gu),
            dma((3, DN_CUT)), dma(dn), dma(dn), dma(dn),
            dma((2, units)), dma((2, units)),
            dma((units,)), dma((units,)),
            dma((units,)), dma((units,)),
        ],
        compiler_params=pltpu.CompilerParams(
            collective_id=0, has_side_effects=True, vmem_limit_bytes=48 * 1024 * 1024
        ),
    )(*[pltpu.with_memory_space_constraint(a, pltpu.HBM) for a in ins])
    serve = jax.ShapeDtypeStruct((1, D, Fl), bf16)
    return pl.pallas_call(
        finish_kernel,
        out_shape=(serve, serve, serve, jax.ShapeDtypeStruct((T, Dq), bf16)),
        in_specs=[vmem] * 3,
        out_specs=(hbm,) * 4,
        scratch_shapes=[dma((4,))],
    )(*[pltpu.with_memory_space_constraint(a, pltpu.VMEM) for a in done])


def solution(mesh):
    shape = mesh.shape
    fits = shape['grp'] == 2 and shape['tp'] == shape['fs'] == 4
    body = fused if fits else local
    placed = (
        P(("grp", "fs"), "tp"),
        P(("grp", "fs"), None),
        P(("grp", "fs"), None),
        P("fs"),
        P(None, "fs", "tp"),
        P(None, "fs", "tp"),
        P(None, "fs", "tp"),
    )
    return jax.shard_map(
        body,
        mesh=mesh,
        in_specs=placed,
        out_specs=(
            P(("grp", "fs"), None, "tp"),
            P(("grp", "fs"), None, "tp"),
            P(("grp", "fs"), None, "tp"),
            P(("grp", "fs"), "tp"),
        ),
        check_vma=False,
    )
```

time: 66.2 us -> 77.2 us (1.17)
  the two profiles are of different devices: /device:TPU:0 before, /device:TPU:6 now
where the time goes in v1:
time: 77.2 us; the launch traced here: 77.1 us
  Pallas kernels  76.4 us (99%)
    pallas_call x1, Pallas kernels, fused(): pl.pallas_call(kernel, out_shape=(pltpu.VMEM((2, D, 2 * Fl), bf16), pltpu...  75.2 us

profile of v1, /device:TPU:6, one launch (start us, length us, event | category | flops | bytes accessed | tf_op | source)
XLA Modules:
  0.0 77.1 jit_solution(5027915808212478080)
XLA Ops:
  0.6 75.2 %shard_map.102 = (bf16[2,2048,256]{2,1,0:T(8,128)(2,1)S(1)}, bf16[2048,256]{1,0:T(8,128)(2,1)S(1)}, bf16[224,512]{1,0:T(8,128)(2,1)S(1)}) custom-call(bf16[224,512]{1,0:T(8,128)(2,1)} %tokens.1, s32[2,224]{1,0:T(2,128)} %bitcast.3, f32[2,224]{1,0:T(2,128)} %bitcast.4, f32[1,512]{1,0:T(1,128)} %bitcast.5, f32[4,512,128]{2,1,0:T(8,128)} %gm.1, ...), custom_call_target="tpu_custom_call" | custom-call | tf_op jit(solution)/shard_map/pallas_call | solution.py:560
  75.8 1.3 %shard_map.103 = (bf16[1,2048,128]{2,1,0:T(8,128)(2,1)}, bf16[1,2048,128]{2,1,0:T(8,128)(2,1)}, bf16[1,2048,128]{2,1,0:T(8,128)(2,1)}, bf16[224,512]{1,0:T(8,128)(2,1)}) custom-call(bf16[2,2048,256]{2,1,0:T(8,128)(2,1)S(1)} %get-tuple-element.7.wgu, bf16[2048,256]{1,0:T(8,128)(2,1)S(1)} %get-tuple-element.8.wd, bf16[224,512]{1,0:T(8,128)(2,1)S(1)} %get-tuple-element.9.moe), custom_call_target="tpu_custom_call" | custom-call | tf_op jit(solution)/shard_map/pallas_call | solution.py:603

commit v2 on v1

--- a/solution.py
+++ b/solution.py
@@ -146,8 +146,8 @@
         pltpu.make_async_copy(ids_h, ids, in_sem.at[2]),
         pltpu.make_async_copy(weights_h, weights, in_sem.at[3]),
     ]
-    small[0].start()
-    small[1].start()
+    for cp in small:
+        cp.start()
     picks = [
         (1 - me, g), (1 - me + 2, g), (me, g), (me + 2, g), (me, 1 - g), (me + 2, 1 - g),
     ]
@@ -161,8 +161,6 @@
             mv.at[m, k], ld_sem.at[m, k],
         )
         loads[k, m].start()
-    small[2].start()
-    small[3].start()
 
     barrier = pltpu.get_barrier_semaphore()
     friends = [to_mate, {"fs": twin}, {"fs": mate_twin}, peer, sib, over]
@@ -173,8 +171,19 @@
     gcol[...] = jnp.transpose(jnp.broadcast_to(gain[...], (Fl, Dl)))
     mine_half = pl.ds(pl.multiple_of(g * H, H), H)
     other_half = pl.ds(pl.multiple_of((1 - g) * H, H), H)
+    small[2].wait()
+    small[3].wait()
+    wrow[me] = jnp.zeros(wsend.shape, f32)
+    wsend[...] = jnp.zeros(wsend.shape, f32)
+    for slot in range(2):
+        for ref, parity in ((wrow.at[me], me), (wsend, 1 - me)):
+            row = jnp.where(ids[...] == parity + 2 * slot, weights[...], 0.0)
+            ref[slot : slot + 1, :T] = jnp.sum(row, axis=0, keepdims=True)
     small[1].wait()
     pl.semaphore_wait(barrier, len(friends))
+    w_hop = remote(wsend, wrow.at[me], w_send, w_recv, to_mate)
+    w_hop.start()
+
 
     def tok(q, rows):
         return xt.at[q, rows, :]
@@ -289,20 +298,6 @@
         loads[4 + slot, 2].wait()
         wd[cut(f, 1 - g, 0, H), lanes] = mv[2, 4 + slot].astype(bf16)
 
-    small[2].wait()
-    small[3].wait()
-    wrow[me] = jnp.zeros(wsend.shape, f32)
-    wsend[...] = jnp.zeros(wsend.shape, f32)
-    for slot in range(2):
-        for ref, parity in ((wrow.at[me], me), (wsend, 1 - me)):
-            row = jnp.where(ids[...] == parity + 2 * slot, weights[...], 0.0)
-            ref[slot : slot + 1, :T] = jnp.sum(row, axis=0, keepdims=True)
-    w_hop = remote(wsend, wrow.at[me], w_send, w_recv, to_mate)
-    w_hop.start()
-
-    remote(tok(t, mate_rows), tok(t, mate_rows), c_send, c_recv, to_mate).wait_recv()
-    spread(mate_rows, 1 - me)
-
     def gu_forward(s, slot, p):
         here = wgu.at[slot, cut(s, g, p, Rg), :]
         remote(here, here, gu_recv.at[s, slot, p], gu_recv.at[s, slot, p], peer).wait_recv()
@@ -329,12 +324,23 @@
     def partial_sums(s, slot):
         return jnp.dot(xt[s], wgu[slot, both(s), :], preferred_element_type=f32)
 
+    gu_all(far_a, 0)
+    gu_all(far_a, 1)
+    remote(tok(t, mate_rows), tok(t, mate_rows), c_send, c_recv, to_mate).wait_recv()
+    spread(mate_rows, 1 - me)
+    pass_on(mine_rows, me)
     gu_all(mate, 0)
-    gu_all(far_a, 0)
-    pass_on(mine_rows, me)
+    gu_all(far_b, 0)
     gu_all(mate, 1)
-    gu_all(far_a, 1)
     pass_on(mate_rows, 1 - me)
+    gu_forward(far_b, 1, 0)
+
+    @pl.when(inner)
+    def _():
+        send_dn((0, 1))
+
+    for p in range(1, GU_CUT):
+        gu_forward(far_b, 1, p)
 
     remote(wsend, wrow.at[1 - me], w_recv, w_recv, to_mate).wait_recv()
     sib_arrived(mine_rows, me)
@@ -356,24 +362,24 @@
 
     for slot in range(2):
         acc[slot] = partial_sums(f, slot)
-    for slot in range(2):
-        for s in (mate, far_a):
+    for s in (far_a, mate):
+        for slot in range(2):
             gu_peer(s, slot)
             acc[slot] += partial_sums(s, slot)
 
-    gu_all(far_b, 0)
-    gu_forward(far_b, 1, 0)
-
-    @pl.when(inner)
-    def _():
-        send_dn((0, 1))
-
-    for p in range(1, GU_CUT):
-        gu_forward(far_b, 1, p)
-    for p in range(DN_CUT):
-        dn_forward(mate, p)
-
-    for slot in range(2):
+    ratio = DN_CUT // per_half
+
+    def far_forward(j):
+        for p in range(j * ratio, (j + 1) * ratio):
+            dn_forward(far_a, p)
+            dn_forward(far_b, p)
+
+    def far_peer(j):
+        for p in range(j * ratio, (j + 1) * ratio):
+            dn_peer(far_a, p)
+            dn_peer(far_b, p)
+
+    def hidden(slot):
         gu_peer(far_b, slot)
         sums = acc[slot] + partial_sums(far_b, slot)
         gate, up = sums[:, :Fl] * inv[...], sums[:, Fl:] * scale[slot]
@@ -392,13 +398,20 @@
         at = pl.ds(u, count)
         return remote(ss.at[n, at], sr.at[n, at], s_send.at[n, u], s_recv.at[n, u], sib)
 
-    def cross(u, count):
-        at = pl.ds(u, count)
-        return remote(xs.at[at], xr.at[at], x_send.at[u], x_recv.at[u], over)
-
-    def back(u, count):
-        at = pl.ds(u, count)
-        return remote(zs.at[at], zr.at[at], z_send.at[u], z_recv.at[u], to_mate)
+    def cross(n, u, j):
+        if x_first(j):
+            return remote(xs.at[n, u], xr.at[n, u], x_send.at[n, u], x_recv.at[n, u], over)
+        half = pl.ds(0, T)
+        return remote(xs.at[n, u, half], xr.at[n, u, half], x_send.at[n, u], x_recv.at[n, u], over)
+
+    def back(n, u):
+        return remote(zs.at[n, u], zr.at[n, u], z_send.at[n, u], z_recv.at[n, u], to_mate)
+
+    def x_first(j):
+        return j % 2 == 0
+
+    def is_kept(n):
+        return home if n == 0 else jnp.logical_not(home)
 
     def theirs(n, s, u, count):
         y = out_part(s, u, count)
@@ -406,83 +419,82 @@
             ss[n, u + j] = y[:, j * Fl : (j + 1) * Fl].astype(bf16)
         swap(n, u, count).start()
 
-    def mine(n, s, u, count):
+    def mine(n, s, u, j0, count):
         y = out_part(s, u, count)
         swap(n, u, count).wait_recv()
-        kept = home if n == 0 else jnp.logical_not(home)
-        parts = [y[:, j * Fl : (j + 1) * Fl] + sr[n, u + j].astype(f32) for j in range(count)]
-
-        @pl.when(kept)
-        def _():
-            for j in range(count):
-                keep[u + j] = parts[j]
-
-        @pl.when(jnp.logical_not(kept))
-        def _():
-            for j in range(count):
-                xs[u + j] = parts[j].astype(bf16)
-            cross(u, count).start()
-
-    def give_back(u, count):
-        cross(u, count).wait_recv()
-        for j in range(count):
-            zs[u + j] = (keep[u + j, mate_rows, :] + xr[u + j, mate_rows, :].astype(f32)).astype(bf16)
-        back(u, count).start()
-
-    def finish(u, count):
-        back(u, count).wait_recv()
-        for j in range(count):
-            lane = (u + j) * Fl
-            lanes = pl.ds(lane if isinstance(lane, int) else pl.multiple_of(lane, Fl), Fl)
-            moe[:, lanes] = (
-                keep[u + j, mine_rows, :] + xr[u + j, mine_rows, :].astype(f32) + zr[u + j].astype(f32)
-            ).astype(bf16)
-
-    ratio = DN_CUT // per_half
-
-    def far_forward(j):
-        for p in range(j * ratio, (j + 1) * ratio):
-            dn_forward(far_a, p)
-            dn_forward(far_b, p)
-
-    def far_peer(j):
-        for p in range(j * ratio, (j + 1) * ratio):
-            dn_peer(far_a, p)
-            dn_peer(far_b, p)
-
+        for i in range(count):
+            j, at = j0 + i, u + i
+            keep[n, at] = y[:, i * Fl : (i + 1) * Fl] + sr[n, at].astype(f32)
+            if x_first(j):
+                @pl.when(jnp.logical_not(is_kept(n)))
+                def _():
+                    xs[n, at] = keep[n, at].astype(bf16)
+                    cross(n, at, j).start()
+            else:
+                zs[n, at] = keep[n, at, mate_rows, :].astype(bf16)
+                back(n, at).start()
+
+    def own(n, u):
+        return keep[n, u, mine_rows, :]
+
+    def second(n, u, j):
+        if x_first(j):
+            @pl.when(is_kept(n))
+            def _():
+                cross(n, u, j).wait_recv()
+                zs[n, u] = (keep[n, u, mate_rows, :] + xr[n, u, mate_rows, :].astype(f32)).astype(bf16)
+                back(n, u).start()
+        else:
+            @pl.when(jnp.logical_not(is_kept(n)))
+            def _():
+                back(n, u).wait_recv()
+                xs[n, u, :T] = (own(n, u) + zr[n, u].astype(f32)).astype(bf16)
+                cross(n, u, j).start()
+
+    def last(n, u, j):
+        back(n, u).wait_recv()
+        if x_first(j):
+            other = xr[n, u, mine_rows, :]
+        else:
+            cross(n, u, j).wait_recv()
+            other = xr[n, u, :T]
+        lanes = pl.ds(pl.multiple_of(u * Fl, Fl), Fl)
+        moe[:, lanes] = (own(n, u) + other.astype(f32) + zr[n, u].astype(f32)).astype(bf16)
+
+    near_units = [(0, u, u % per_half) for u in range(units)]
+    far_units = [(1, half * per_half + j, j) for half in (g, 1 - g) for j in range(per_half)]
+
+    for p in range(DN_CUT):
+        dn_forward(mate, p)
+    hidden(0)
+    far_forward(0)
+    hidden(1)
     for p in range(DN_CUT):
         dn_peer(mate, p)
-    for h in range(2):
-        theirs(0, near_theirs, h * per_half, per_half)
-    for h in range(2):
-        mine(0, near_mine, h * per_half, per_half)
-
-    for j in range(per_half):
-        far_forward(j)
-        for half in (g, 1 - g):
-            u = half * per_half + j
-            if half is not g:
-                far_peer(j)
-            theirs(1, far_theirs, u, 1)
-            mine(1, far_mine, u, 1)
-        if j == 0:
-            @pl.when(home)
-            def _():
-                for h in range(2):
-                    give_back(h * per_half, per_half)
-
-    @pl.when(home)
-    def _():
-        for h in range(2):
-            finish(h * per_half, per_half)
-
-    @pl.when(jnp.logical_not(home))
-    def _():
-        order = [half * per_half + j for j in range(per_half) for half in (g, 1 - g)]
-        for u in order:
-            give_back(u, 1)
-        for u in order:
-            finish(u, 1)
+    for half in range(2):
+        theirs(0, near_theirs, half * per_half, per_half)
+    far_forward(1)
+    for half in range(2):
+        mine(0, near_mine, half * per_half, 0, per_half)
+    for n, u, j in far_units[:per_half]:
+        theirs(1, far_theirs, u, 1)
+    for n, u, j in far_units[:per_half]:
+        mine(1, far_mine, u, j, 1)
+    for half, (n, u, j) in zip(range(per_half), far_units[per_half:]):
+        far_peer(half)
+        theirs(1, far_theirs, u, 1)
+    for half, (n, u, j) in zip(range(per_half), far_units[per_half:]):
+        mine(1, far_mine, u, j, 1)
+    for half_units in near_units + far_units:
+        second(*half_units)
+    for half_units in far_units:
+        @pl.when(jnp.logical_not(home))
+        def _():
+            last(*half_units)
+    for half_units in near_units:
+        @pl.when(home)
+        def _():
+            last(*half_units)
 
     token_hop.wait_send()
     w_hop.wait_send()
@@ -505,24 +517,21 @@
         for p in range(DN_CUT):
             here = wd.at[cut(s, g, p, Rd), :]
             remote(here, here, dny_send.at[s, p], dny_send.at[s, p], peer).wait_send()
-    for h in range(2):
-        swap(0, h * per_half, per_half).wait_send()
+    for half in range(2):
+        swap(0, half * per_half, per_half).wait_send()
     for u in range(units):
         swap(1, u, 1).wait_send()
-
-    @pl.when(home)
-    def _():
+    for n in range(2):
         for u in range(units):
-            cross(u, 1).wait_send()
-        for h in range(2):
-            back(h * per_half, per_half).wait_send()
-
-    @pl.when(jnp.logical_not(home))
-    def _():
-        for h in range(2):
-            cross(h * per_half, per_half).wait_send()
-        for u in range(units):
-            back(u, 1).wait_send()
+            j = u % per_half
+
+            @pl.when(is_kept(n) | (not x_first(j)))
+            def _():
+                back(n, u).wait_send()
+
+            @pl.when(jnp.logical_not(is_kept(n)))
+            def _():
+                cross(n, u, j).wait_send()
 
 
 def finish_kernel(wgu, wd, moe, gate_o, up_o, down_o, moe_o, sems):
@@ -581,19 +590,19 @@
             pltpu.VMEM((2 * T, 2 * Fl), bf16),
             pltpu.VMEM((2, units, 2 * T, Fl), bf16),
             pltpu.VMEM((2, units, 2 * T, Fl), bf16),
-            pltpu.VMEM((units, 2 * T, Fl), bf16),
-            pltpu.VMEM((units, 2 * T, Fl), bf16),
-            pltpu.VMEM((units, 2 * T, Fl), f32),
-            pltpu.VMEM((units, T, Fl), bf16),
-            pltpu.VMEM((units, T, Fl), bf16),
+            pltpu.VMEM((2, units, 2 * T, Fl), bf16),
+            pltpu.VMEM((2, units, 2 * T, Fl), bf16),
+            pltpu.VMEM((2, units, 2 * T, Fl), f32),
+            pltpu.VMEM((2, units, T, Fl), bf16),
+            pltpu.VMEM((2, units, T, Fl), bf16),
             dma((4,)), dma((3, 6)),
             dma(()), dma(()), dma(()), dma(()),
             dma((NT, 2)), dma((2,)), dma((NT, 2)),
             dma((3, 2, GU_CUT)), dma(gu), dma(gu), dma(gu),
             dma((3, DN_CUT)), dma(dn), dma(dn), dma(dn),
             dma((2, units)), dma((2, units)),
-            dma((units,)), dma((units,)),
-            dma((units,)), dma((units,)),
+            dma((2, units)), dma((2, units)),
+            dma((2, units)), dma((2, units)),
         ],
         compiler_params=pltpu.CompilerParams(
             collective_id=0, has_side_effects=True, vmem_limit_bytes=48 * 1024 * 1024

time: 77.2 us -> 55.5 us (0.72)
  the two profiles are of different devices: /device:TPU:6 before, /device:TPU:0 now
where the time goes in v2:
time: 55.5 us; the launch traced here: 55.3 us
  Pallas kernels  54.7 us (99%)
  between operations  0.64 us (1%)
    pallas_call x1, Pallas kernels, fused(): pl.pallas_call(kernel, out_shape=(pltpu.VMEM((2, D, 2 * Fl), bf16), pltpu...  53.4 us
    pallas_call x1, Pallas kernels, fused(): pl.pallas_call(finish_kernel, out_shape=(serve, serve, serve, jax.ShapeDt...  1.26 us

profile of v2, /device:TPU:0, one launch (start us, length us, event | category | flops | bytes accessed | tf_op | source)
XLA Modules:
  0.0 55.3 jit_solution(14470915093095065291)
XLA Ops:
  0.6 53.4 %shard_map.102 = (bf16[2,2048,256]{2,1,0:T(8,128)(2,1)S(1)}, bf16[2048,256]{1,0:T(8,128)(2,1)S(1)}, bf16[224,512]{1,0:T(8,128)(2,1)S(1)}) custom-call(bf16[224,512]{1,0:T(8,128)(2,1)} %tokens.1, s32[2,224]{1,0:T(2,128)} %bitcast.3, f32[2,224]{1,0:T(2,128)} %bitcast.4, f32[1,512]{1,0:T(1,128)} %bitcast.5, f32[4,512,128]{2,1,0:T(8,128)} %gm.1, ...), custom_call_target="tpu_custom_call" | custom-call | tf_op jit(solution)/shard_map/pallas_call | solution.py:569
  54.1 1.3 %shard_map.103 = (bf16[1,2048,128]{2,1,0:T(8,128)(2,1)}, bf16[1,2048,128]{2,1,0:T(8,128)(2,1)}, bf16[1,2048,128]{2,1,0:T(8,128)(2,1)}, bf16[224,512]{1,0:T(8,128)(2,1)}) custom-call(bf16[2,2048,256]{2,1,0:T(8,128)(2,1)S(1)} %get-tuple-element.7.wgu, bf16[2048,256]{1,0:T(8,128)(2,1)S(1)} %get-tuple-element.8.wd, bf16[224,512]{1,0:T(8,128)(2,1)S(1)} %get-tuple-element.9.moe), custom_call_target="tpu_custom_call" | custom-call | tf_op jit(solution)/shard_map/pallas_call | solution.py:612
